TPU v7x, 256 devices: a 4x2x16 block of a 4x16x16 slice. The times are simulated.
256 devices in a mesh: grp: 2 (over y), sp: 16 (over z), tp: 8 (over x, core).
Axes of the slice: x: 4, y: 2, z: 16, core: 2. Of those that a mesh axis runs over, the one named last changes fastest.
The devices are a block of a 4x16x16 slice.
Arguments:
- queries: bfloat16 [24576, 1024], P(('grp', 'sp'), 'tp'), parts along dimension 0, may hold values from -200 to 200
- key_rows: bfloat16 [24576, 512], P(('grp', 'sp'), 'tp'), parts along dimension 0, may hold values from -6 to 6
- value_rows: bfloat16 [24576, 512], P(('grp', 'sp'), 'tp'), parts along dimension 0, may hold values from -6 to 6
- doc_ids: int32 [24576], P(('grp', 'sp')), parts along dimension 0, may hold values from 0 to 7, never falling along the last dimension, each value on 1 to 3072 neighbouring positions
- sink_logits: float32 [16], P('tp'), may hold values from 2 to 7
- out_weight: bfloat16 [1024, 2048], P('tp', 'sp'), may hold values from -0.1875 to 0.1875
- residual: bfloat16 [24576, 2048], P(('grp', 'sp', 'tp')), parts along dimension 0, may hold values from -6 to 6
- gain_mixed: float32 [2048], replicated, may hold values from 0.1 to 1.9
- gain_before: float32 [2048], replicated, may hold values from 0.1 to 1.9
- gain_after: float32 [2048], replicated, may hold values from 0.1 to 1.9
- gate_weight: bfloat16 [2048, 6144], P('sp', 'tp'), may hold values from -0.125 to 0.125
- up_weight: bfloat16 [2048, 6144], P('sp', 'tp'), may hold values from -0.125 to 0.125
- down_weight: bfloat16 [6144, 2048], P('tp', 'sp'), may hold values from -0.078125 to 0.078125
Outputs:
- layer_out: bfloat16 [24576, 2048], P(('grp', 'sp', 'tp')), parts along dimension 0
There are 2 independent parts, one for each index of `grp`. A program takes and returns all parts, laid end to end along the dimension named above; an argument that names none is the same for every part. Nothing has to cross between parts.
All inputs are finite; a program needn't handle non-finite values.
Results may differ from a plain program's by a relative error of at most 0.015.
Values may be sent and summed in bfloat16 or wider, within the bound.
A program may use at most 128 MiB of HBM per device.

v0:
```python
import jax
import jax.numpy as jnp
from jax import lax
from jax.sharding import PartitionSpec as P

HEAD_DIM = 64
WINDOW = 128
epsilon = 1e-06
masked_value = -1e30


def passed_along(value, axis, steps):
    count = lax.axis_size(axis)
    first, last = (max(0, -steps), min(count, count - steps))
    return lax.ppermute(value, axis, [(source, source + steps) for source in range(first, last)])


def from_everyone(shard, axis):
    size = lax.axis_size(axis)
    return lax.all_to_all(
        jnp.broadcast_to(shard[None], (size, *shard.shape)), axis, 0, 0, tiled=True
    )


def laid_out(pieces, dim):
    pieces = jnp.moveaxis(pieces, 0, dim)
    lengths = pieces.shape
    return pieces.reshape(*lengths[:dim], lengths[dim] * lengths[dim + 1], *lengths[dim + 2 :])


def gather_directly(shard, axis, dim):
    pieces = from_everyone(shard, axis)
    return laid_out(pieces, dim)


def turned_gather(arrays, axis, dims):
    turned = [jnp.moveaxis(a, dim, 0) for a, dim in zip(arrays, dims)]
    both = jnp.concatenate([t.reshape(len(t), -1) for t in turned], axis=1)
    filled, at, finished = (lax.all_gather(both, axis, axis=0, tiled=True), 0, [])
    for t, dim in zip(turned, dims):
        piece = filled[:, at : at + t[0].size].reshape(-1, *t.shape[1:])
        finished.append(jnp.moveaxis(piece, 0, dim))
        at += t[0].size
    return tuple(finished)


def split_up(shard, dim, size):
    lengths = shard.shape
    pieces = shard.reshape(*lengths[:dim], size, lengths[dim] // size, *lengths[dim + 1 :])
    return jnp.moveaxis(pieces, dim, 0)


def summed_on_arrival(shard, axis, dim):
    size = lax.axis_size(axis)
    pieces = lax.all_to_all(split_up(shard, dim, size), axis, 0, 0, tiled=True)
    return jnp.sum(pieces.astype(jnp.float32), axis=0)


def stored(value):
    return lax.optimization_barrier(value.astype(jnp.bfloat16)).astype(jnp.float32)


def rms_scaled(value, gain):
    return value * lax.rsqrt(jnp.mean(value * value, axis=-1, keepdims=True) + epsilon) * gain


def windows(array, blocks):
    first = array[:-WINDOW].reshape((blocks, WINDOW) + array.shape[1:])
    second = array[WINDOW:].reshape((blocks, WINDOW) + array.shape[1:])
    return jnp.concatenate([first, second], axis=1)


def attend(queries, key_rows, value_rows, doc_ids, sink_logits):
    length = queries.shape[0]
    blocks = length // WINDOW
    local_kv = key_rows.shape[1] // HEAD_DIM
    group_size = queries.shape[1] // HEAD_DIM // local_kv
    offset = lax.axis_index("sp") * length
    tail_keys, tail_values, tail_docs = passed_along(
        (key_rows[length - WINDOW :], value_rows[length - WINDOW :], doc_ids[length - WINDOW :]),
        "sp",
        1,
    )
    key_blocks = windows(jnp.concatenate([tail_keys, key_rows], axis=0), blocks).reshape(
        blocks, 2 * WINDOW, local_kv, HEAD_DIM
    )
    value_blocks = windows(jnp.concatenate([tail_values, value_rows], axis=0), blocks).reshape(
        blocks, 2 * WINDOW, local_kv, HEAD_DIM
    )
    key_docs = windows(jnp.concatenate([tail_docs, doc_ids], axis=0), blocks)
    key_places = windows(offset - WINDOW + jnp.arange(length + WINDOW, dtype=jnp.int32), blocks)
    query_places = (offset + jnp.arange(length, dtype=jnp.int32)).reshape(blocks, WINDOW)
    query_docs = doc_ids.reshape(blocks, WINDOW)
    query_blocks = queries.reshape(blocks, WINDOW, local_kv, group_size, HEAD_DIM)
    scores = jnp.einsum(
        "bqhgd,bkhd->bhgqk", query_blocks, key_blocks, preferred_element_type=jnp.float32
    ) * HEAD_DIM ** (-0.5)
    distance = query_places[:, :, None] - key_places[:, None, :]
    valid = (distance >= 0) & (distance < WINDOW) & (key_places[:, None, :] >= 0)
    valid = valid & (query_docs[:, :, None] == key_docs[:, None, :])
    scores = jnp.where(valid[:, None, None], scores, masked_value)
    sinks = sink_logits.reshape(local_kv, group_size)[None, :, :, None]
    top = jnp.maximum(jnp.max(scores, axis=-1), sinks)
    weight = jnp.exp(scores - top[..., None])
    denom = jnp.sum(weight, axis=-1) + jnp.exp(sinks - top)
    summed = jnp.einsum(
        "bhgqk,bkhd->bqhgd",
        weight.astype(jnp.bfloat16),
        value_blocks,
        preferred_element_type=jnp.float32,
    )
    scale = jnp.transpose(denom, (0, 3, 1, 2))[..., None]
    return (summed / scale).reshape(length, queries.shape[1]).astype(jnp.bfloat16)


def per_device(
    queries,
    key_rows,
    value_rows,
    doc_ids,
    sink_logits,
    out_weight,
    residual,
    gain_mixed,
    gain_before,
    gain_after,
    gate_weight,
    up_weight,
    down_weight,
):
    mixed = attend(queries, key_rows, value_rows, doc_ids, sink_logits)
    head_columns = gather_directly(out_weight, "sp", 1)
    by_rows = lax.all_to_all(mixed, "tp", split_axis=0, concat_axis=1, tiled=True)
    projected = jnp.dot(
        by_rows,
        lax.all_gather(head_columns, "tp", axis=0, tiled=True),
        preferred_element_type=jnp.float32,
    )
    projected = stored(projected)
    after = stored(residual.astype(jnp.float32) + rms_scaled(projected, gain_mixed))
    normed = rms_scaled(after, gain_before).astype(jnp.bfloat16)
    full_gate, full_up, full_down = turned_gather(
        (gate_weight, up_weight, down_weight), "sp", (0, 0, 1)
    )
    piece = lax.all_gather(normed, "tp", axis=0, tiled=True)
    gate = jnp.dot(piece, full_gate, preferred_element_type=jnp.float32)
    upward = jnp.dot(piece, full_up, preferred_element_type=jnp.float32)
    hidden = (jax.nn.silu(gate) * upward).astype(jnp.bfloat16)
    ffn_out = stored(
        summed_on_arrival(
            jnp.dot(hidden, full_down, preferred_element_type=jnp.float32).astype(jnp.bfloat16),
            "tp",
            0,
        )
    )
    return (after + 0.5 * rms_scaled(ffn_out, gain_after)).astype(jnp.bfloat16)


def solution(mesh):
    return jax.shard_map(
        per_device,
        mesh=mesh,
        in_specs=(
            P(("grp", "sp"), "tp"),
            P(("grp", "sp"), "tp"),
            P(("grp", "sp"), "tp"),
            P(("grp", "sp")),
            P("tp"),
            P("tp", "sp"),
            P(("grp", "sp", "tp"), None),
            P(),
            P(),
            P(),
            P("sp", "tp"),
            P("sp", "tp"),
            P("tp", "sp"),
        ),
        out_specs=P(("grp", "sp", "tp"), None),
        check_vma=False,
    )
```

profile of v0, /device:TPU:33, one launch (start us, length us, event | category | flops | bytes accessed | tf_op | source)
XLA Modules:
  0.0 348.9 jit_solution(4281266326615611289)
XLA Ops:
  6.6 1.0 copy.40
  7.7 47.2 %all_to_all.26 = bf16[16,128,128]{1,2,0:T(8,128)(2,1)} all-to-all(bf16[16,128,128]{1,2,0:T(8,128)(2,1)S(1)} %broadcast_in_dim.16), channel_id=1, replica_groups=mesh['grp'=2,'sp'=16,'tp'=8] {'sp'}, dimensions={0} | all-to-all | bytes 1048576 | tf_op jit(solution)/shard_map/all_to_all | solution.py:20
  55.0 0.7 slice.49
  55.7 5.3 %collective-permute-start.1 = (s32[128]{0:T(128)S(1)}, s32[128]{0:T(128)S(1)}, u32[]{:S(2)}, u32[]{:S(2)}) collective-permute-start(s32[128]{0:T(128)S(1)} %slice.49), channel_id=1, source_target_pairs={{0,8},{8,16},{16,24},{24,32},{32,40},{40,48},{48,56},{56,64},{64,7... | collective-permute-start | bytes 1544 | tf_op jit(solution)/shard_map/ppermute | solution.py:15
  61.0 0.7 slice.45
  61.7 2.2 collective-permute-start
  63.9 0.7 slice.52
  64.6 4.6 %collective-permute-start.2 = (bf16[128,64]{0,1:T(8,128)(2,1)S(1)}, bf16[128,64]{0,1:T(8,128)(2,1)S(1)}, u32[]{:S(2)}, u32[]{:S(2)}) collective-permute-start(bf16[128,64]{0,1:T(8,128)(2,1)S(1)} %slice.52), channel_id=1, source_target_pairs={{0,8},{8,16},{16,24},{24,32},{32,40},{40,48},{48,56},{56,64},{64,7... | collective-permute-start | bytes 49160 | tf_op jit(solution)/shard_map/ppermute | solution.py:15
  69.6 1.0 fusion.30
  70.6 0.5 fusion.48
  71.9 0.4 copy.48
  72.5 17.5 %all_to_all.27 = bf16[8,96,128]{2,1,0:T(8,128)(2,1)S(1)} all-to-all(bf16[8,96,128]{2,1,0:T(8,128)(2,1)S(1)} %reshape.171), channel_id=1, replica_groups=mesh['grp'=2,'sp'=16,'tp'=8] {'tp'}, dimensions={0} | all-to-all | bytes 393216 | tf_op jit(solution)/shard_map/all_to_all | solution.py:133
  90.0 12.1 %all-gather.4.cloned.1.call-done = bf16[1024,2048]{0,1:T(8,128)(2,1)} async-done(((bf16[128,2048]{0,1:T(8,128)(2,1)}), bf16[1024,2048]{0,1:T(8,128)(2,1)}) %all-gather.4.cloned.1.call-update) | async-done | bytes 4194320 | tf_op jit(solution)/shard_map/all_gather | solution.py:136
  102.2 3.6 %convolution_convert_fusion.1 = bf16[96,2048]{1,0:T(8,128)(2,1)S(1)} fusion(bf16[1024,2048]{0,1:T(8,128)(2,1)} %all-gather.4.cloned.1.call-done, bf16[8,96,128]{2,1,0:T(8,128)(2,1)S(1)} %all_to_all.27), kind=kOutput, calls=%fused_computation.7 | convolution fusion | flops 402849792 | bytes 4784128 | tf_op jit(solution)/shard_map/dot_general | solution.py:134
  106.4 0.9 fusion.23
  108.0 0.9 pad_maximum_fusion
  108.9 31.3 %all-gather.6.cloned.1.call-done = bf16[768,2048]{1,0:T(8,128)(2,1)} async-done(((bf16[96,2048]{1,0:T(8,128)(2,1)}), bf16[768,2048]{1,0:T(8,128)(2,1)}) %all-gather.6.cloned.1.call-update) | async-done | bytes 3145744 | tf_op jit(solution)/shard_map/all_gather | solution.py:145
  140.2 128.3 %all-gather.8.cloned.1.call-done = bf16[2048,2304]{0,1:T(8,128)(2,1)} async-done(((bf16[128,2304]{0,1:T(8,128)(2,1)}), bf16[2048,2304]{0,1:T(8,128)(2,1)}) %all-gather.8.cloned.1.call-update) | async-done | bytes 9437200 | tf_op jit(solution)/shard_map/all_gather | solution.py:39
  268.5 6.9 %fusion.3 = f32[768,768]{1,0:T(8,128)} fusion(bf16[768,2048]{1,0:T(8,128)(2,1)} %all-gather.6.cloned.1.call-done, bf16[2048,2304]{0,1:T(8,128)(2,1)} %all-gather.8.cloned.1.call-done), kind=kOutput, calls=%fused_computation.4 | convolution fusion | flops 2415919104 | bytes 8650752 | tf_op jit(solution)/shard_map/dot_general | solution.py:146
  275.4 11.0 %convolution_convert_fusion = bf16[768,2048]{1,0:T(8,128)(2,1)} fusion(bf16[2048,2304]{0,1:T(8,128)(2,1)} %all-gather.8.cloned.1.call-done, f32[768,768]{1,0:T(8,128)} %fusion.3, bf16[768,2048]{1,0:T(8,128)(2,1)S(1)} %copy-done.12), kind=kOutput, calls=%fused_computation | convolution fusion | flops 4836950016 | bytes 14942208 | tf_op jit(solution)/shard_map/dot_general | solution.py:151
  286.4 51.4 %all_to_all.28 = bf16[8,96,2048]{2,1,0:T(8,128)(2,1)S(1)} all-to-all(bf16[8,96,2048]{2,1,0:T(8,128)(2,1)} %bitcast.84), channel_id=1, replica_groups=mesh['grp'=2,'sp'=16,'tp'=8] {'tp'}, dimensions={0} | all-to-all | bytes 6291456 | tf_op jit(solution)/shard_map/all_to_all | solution.py:55
  337.7 1.4 reduce_sum.54
  339.2 1.2 fusion.18
  340.4 2.0 fusion.24
  (61 shorter events, 2.8 us)
Async XLA Ops:
  6.5 63.0 %copy-start.7 = (s32[768]{0:T(1024)S(1)}, s32[768]{0:T(1024)}, u32[]{:S(2)}) copy-start(s32[768]{0:T(1024)} %param.16) | copy-start | bytes 9220
  6.5 62.7 %copy-start.1 = (bf16[768,64]{0,1:T(8,128)(2,1)S(1)}, bf16[768,64]{0,1:T(8,128)(2,1)}, u32[]{:S(2)}) copy-start(bf16[768,64]{0,1:T(8,128)(2,1)} %param.15) | copy-start | bytes 294916
  6.6 62.7 %copy-start = (bf16[768,64]{0,1:T(8,128)(2,1)S(1)}, bf16[768,64]{0,1:T(8,128)(2,1)}, u32[]{:S(2)}) copy-start(bf16[768,64]{0,1:T(8,128)(2,1)} %param.14) | copy-start | bytes 294916
  6.6 62.8 %copy-start.6 = (bf16[768,128]{1,0:T(8,128)(2,1)S(1)}, bf16[768,128]{1,0:T(8,128)(2,1)}, u32[]{:S(2)}) copy-start(bf16[768,128]{1,0:T(8,128)(2,1)} %param.13) | copy-start | bytes 589828
  6.6 95.6 %all-gather.4.cloned.1.call-start = ((), (), s32[]{:S(2)}) async-start(), calls=%async_computation.3 | async-start | bytes 4718592 | tf_op jit(solution)/shard_map/all_gather | solution.py:136
  54.9 16.2 %copy-start.11 = (f32[2]{0:T(128)S(1)}, f32[2]{0:T(128)}, u32[]{:S(2)}) copy-start(f32[2]{0:T(128)} %param.17) | copy-start | bytes 28
  54.9 85.2 %all-gather.6.cloned.1.call-start = ((), (), s32[]{:S(2)}) async-start(), calls=%async_computation.4 | async-start | bytes 3538944 | tf_op jit(solution)/shard_map/all_gather | solution.py:145
  55.7 13.8 %collective-permute-start.1 = (s32[128]{0:T(128)S(1)}, s32[128]{0:T(128)S(1)}, u32[]{:S(2)}, u32[]{:S(2)}) collective-permute-start(s32[128]{0:T(128)S(1)} %slice.49), channel_id=1, source_target_pairs={{0,8},{8,16},{16,24},{24,32},{32,40},{40,48},{48,56},{56,64},{64,7... | collective-permute-start | bytes 1544 | tf_op jit(solution)/shard_map/ppermute | solution.py:15
  61.7 8.9 %collective-permute-start = (bf16[128,64]{0,1:T(8,128)(2,1)S(1)}, bf16[128,64]{0,1:T(8,128)(2,1)S(1)}, u32[]{:S(2)}, u32[]{:S(2)}) collective-permute-start(bf16[128,64]{0,1:T(8,128)(2,1)S(1)} %slice.45), channel_id=1, source_target_pairs={{0,8},{8,16},{16,24},{24,32},{32,40},{40,48},{48,56},{56,64},{64,7... | collective-permute-start | bytes 49160 | tf_op jit(solution)/shard_map/ppermute | solution.py:15
  64.6 5.9 %collective-permute-start.2 = (bf16[128,64]{0,1:T(8,128)(2,1)S(1)}, bf16[128,64]{0,1:T(8,128)(2,1)S(1)}, u32[]{:S(2)}, u32[]{:S(2)}) collective-permute-start(bf16[128,64]{0,1:T(8,128)(2,1)S(1)} %slice.52), channel_id=1, source_target_pairs={{0,8},{8,16},{16,24},{24,32},{32,40},{40,48},{48,56},{56,64},{64,7... | collective-permute-start | bytes 49160 | tf_op jit(solution)/shard_map/ppermute | solution.py:15
  90.0 16.0 %copy-start.2 = (bf16[96,2048]{1,0:T(8,128)(2,1)S(1)}, bf16[96,2048]{1,0:T(8,128)(2,1)}, u32[]{:S(2)}) copy-start(bf16[96,2048]{1,0:T(8,128)(2,1)} %param.19) | copy-start | bytes 1179652
  90.0 16.0 %copy-start.8 = (f32[2048]{0:T(1024)S(1)}, f32[2048]{0:T(1024)}, u32[]{:S(2)}) copy-start(f32[2048]{0:T(1024)} %param.20) | copy-start | bytes 24580
  90.0 16.4 %copy-start.9 = (f32[2048]{0:T(1024)S(1)}, f32[2048]{0:T(1024)}, u32[]{:S(2)}) copy-start(f32[2048]{0:T(1024)} %param.21) | copy-start | bytes 24580
  105.8 1.9 copy-start.4
  105.8 2.0 copy-start.5
  105.8 2.2 copy-start.3
  107.4 161.1 %all-gather.8.cloned.1.call-start = ((), (), s32[]{:S(2)}) async-start(), calls=%async_computation.5 | async-start | bytes 10027008 | tf_op jit(solution)/shard_map/all_gather | solution.py:39
  140.2 135.2 %copy-start.12 = (bf16[768,2048]{1,0:T(8,128)(2,1)S(1)}, bf16[768,2048]{1,0:T(8,128)(2,1)}, u32[]{:S(2)}) copy-start(bf16[768,2048]{1,0:T(8,128)(2,1)} %all-gather.6.cloned.1.call-done) | copy-start | bytes 9437188
  337.7 2.6 copy-start.10
Sparse Core Ops, SparseCore 0:
  55.1 47.0 all-gather.3
  107.5 32.6 all-gather.5
  141.9 126.5 all-gather.7
where the time goes:
time: 349 us
  waiting for transfers between devices  172 us (49%)
  blocking collectives  116 us (33%)
  matrix products  22.3 us (6%)
  between operations  13.5 us (4%)
  starting transfers between devices  12.4 us (4%)
  other arithmetic  8.34 us (2%)
  local copies, waits for them, and re-layouts  4.39 us (1%)
    all_gather x1, waiting for transfers between devices, turned_gather(): lax.all_gather(both, axis, axis=0, tiled=True)  128 us
    all_to_all x1, blocking collectives, summed_on_arrival(): pieces = lax.all_to_all(split_up(shard, dim, size), axis, 0, 0, tiled=True)  51.4 us
    all_to_all x1, blocking collectives, from_everyone(): lax.all_to_all(jnp.broadcast_to(shard[None], (size, *shard.shape)), axis,...  47.2 us
    all_gather x1, waiting for transfers between devices, per_device(): piece = lax.all_gather(normed, 'tp', axis=0, tiled=True)  31.3 us
    all_to_all x1, blocking collectives, per_device(): lax.all_to_all(mixed, 'tp', split_axis=0, concat_axis=1, tiled=True)  17.5 us
    all_gather x1, waiting for transfers between devices, per_device(): lax.all_gather(head_columns, 'tp', axis=0, tiled=True)  12.1 us
    ppermute x3, starting transfers between devices, passed_along(): lax.ppermute(value, axis, [(source, source + steps) for source in range(f...  12 us
    dot_general x1, matrix products, per_device(): jnp.dot(hidden, full_down, preferred_element_type=jnp.float32)  11 us
  transfers between devices with their start and end apart: 6, of which 3 were waited for; matrix products, arithmetic and copies ran while one was open for 2% of the time, Pallas kernels for 0%

commit v1 on v0

--- a/solution.py
+++ b/solution.py
@@ -36,7 +36,13 @@
 def turned_gather(arrays, axis, dims):
     turned = [jnp.moveaxis(a, dim, 0) for a, dim in zip(arrays, dims)]
     both = jnp.concatenate([t.reshape(len(t), -1) for t in turned], axis=1)
-    filled, at, finished = (lax.all_gather(both, axis, axis=0, tiled=True), 0, [])
+    filled, at, finished = (
+        jnp.concatenate(
+            lax.all_to_all(jnp.stack(lax.axis_size(axis) * [both], 0), axis, 0, 0), axis=0
+        ),
+        0,
+        [],
+    )
     for t, dim in zip(turned, dims):
         piece = filled[:, at : at + t[0].size].reshape(-1, *t.shape[1:])
         finished.append(jnp.moveaxis(piece, 0, dim))

time: 349 us -> 585 us (1.68)
  waiting for transfers between devices: 172 us -> 429 us
  blocking collectives: 116 us -> 42.4 us
  starting transfers between devices: 12.4 us -> 53.1 us
  local copies, waits for them, and re-layouts: 4.39 us -> 12.6 us
    all_to_all x0 -> x3, waiting for transfers between devices: none -> 349 us  [the longest x1 321 us: turned_gather(): lax.all_to_all(jnp.stack(lax.axis_size(axis) * [both], 0), axis, 0, 0)]
    all_gather x1 -> x0, waiting for transfers between devices: 128 us -> none  [turned_gather(): lax.all_gather(both, axis, axis=0, tiled=True)]
    all_to_all x2 -> x0, blocking collectives: 64.7 us -> none  [the longest x1 47.2 us: from_everyone(): lax.all_to_all(jnp.broadcast_to(shard[None], (size, *shard.shape)), axis,...]
    all_to_all x0 -> x3, starting transfers between devices: none -> 38.7 us  [the longest x1 13.5 us: per_device(): lax.all_to_all(mixed, 'tp', split_axis=0, concat_axis=1, tiled=True)]
    all_gather x1, waiting for transfers between devices: 12.1 us -> 44 us  [per_device(): lax.all_gather(head_columns, 'tp', axis=0, tiled=True)]
    all_to_all x1, blocking collectives: 51.4 us -> 42.4 us  [summed_on_arrival(): pieces = lax.all_to_all(split_up(shard, dim, size), axis, 0, 0, tiled=True)]
  transfers between devices with their start and end apart: 6 -> 8, of which waited for: 3 -> 5; matrix products, arithmetic and copies ran while one was open for 2% -> 3% of each run, Pallas kernels for 0% -> 0%
where the time goes in v1:
time: 585 us; the launch traced here: 584 us
  waiting for transfers between devices  429 us (73%)
  starting transfers between devices  53.1 us (9%)
  blocking collectives  42.4 us (7%)
  matrix products  22.4 us (4%)
  between operations  13.8 us (2%)
  local copies, waits for them, and re-layouts  12.6 us (2%)
  other arithmetic  10.5 us (2%)
    all_to_all x1, waiting for transfers between devices, turned_gather(): lax.all_to_all(jnp.stack(lax.axis_size(axis) * [both], 0), axis, 0, 0)  321 us
    all_gather x1, waiting for transfers between devices, per_device(): lax.all_gather(head_columns, 'tp', axis=0, tiled=True)  44 us
    all_to_all x1, blocking collectives, summed_on_arrival(): pieces = lax.all_to_all(split_up(shard, dim, size), axis, 0, 0, tiled=True)  42.4 us
    all_gather x1, waiting for transfers between devices, per_device(): piece = lax.all_gather(normed, 'tp', axis=0, tiled=True)  34.9 us
    all_to_all x1, waiting for transfers between devices, from_everyone(): lax.all_to_all(jnp.broadcast_to(shard[None], (size, *shard.shape)), axis,...  22.2 us
    ppermute x3, starting transfers between devices, passed_along(): lax.ppermute(value, axis, [(source, source + steps) for source in range(f...  14.1 us
    all_to_all x1, starting transfers between devices, per_device(): lax.all_to_all(mixed, 'tp', split_axis=0, concat_axis=1, tiled=True)  13.5 us
    all_to_all x1, starting transfers between devices, from_everyone(): lax.all_to_all(jnp.broadcast_to(shard[None], (size, *shard.shape)), axis,...  13 us
  transfers between devices with their start and end apart: 8, of which 5 were waited for; matrix products, arithmetic and copies ran while one was open for 3% of the time, Pallas kernels for 0%

profile of v1, /device:TPU:33, one launch (start us, length us, event | category | flops | bytes accessed | tf_op | source)
XLA Modules:
  0.0 583.7 jit_solution(6348786215243899382)
XLA Ops:
  7.3 5.2 collective-permute-start.2
  13.2 4.4 collective-permute-start.1
  18.4 4.4 collective-permute-start
  22.8 0.9 copy_bitcast_fusion
  23.7 0.9 copy_bitcast_fusion.2
  24.7 1.1 reshape.176
  27.3 1.7 fusion.30
  32.5 13.5 %all-to-all-start = ((bf16[8,96,128]{2,1,0:T(8,128)(2,1)}), bf16[8,96,128]{2,1,0:T(8,128)(2,1)S(1)}, u32[]{:S(2)}, u32[]{:S(2)}) async-start(bf16[8,96,128]{2,1,0:T(8,128)(2,1)} %reshape.177), calls=%async_computation | async-start | bytes 393216 | tf_op jit(solution)/shard_map/all_to_all | solution.py:139
  46.1 5.8 all-to-all-done
  52.8 13.0 %all-to-all-start.1 = ((bf16[16,128,128]{1,2,0:T(8,128)(2,1)}), bf16[16,128,128]{1,2,0:T(8,128)(2,1)S(1)}, u32[]{:S(2)}, u32[]{:S(2)}) async-start(bf16[16,128,128]{1,2,0:T(8,128)(2,1)} %broadcast_in_dim.16), calls=%async_computation.1 | async-start | bytes 1048576 | tf_op jit(solution)/shard_map/all_to_all | solution.py:20
  66.5 22.2 %all-to-all-done.1 = bf16[16,128,128]{1,2,0:T(8,128)(2,1)S(1)} async-done(((bf16[16,128,128]{1,2,0:T(8,128)(2,1)}), bf16[16,128,128]{1,2,0:T(8,128)(2,1)S(1)}, u32[]{:S(2)}, u32[]{:S(2)}) %all-to-all-start.1) | async-done | bytes 524320 | tf_op jit(solution)/shard_map/all_to_all | solution.py:20
  88.7 4.6 stack.2
  93.3 12.2 %all-to-all-start.2 = ((bf16[16,128,2304]{2,1,0:T(8,128)(2,1)}), bf16[16,128,2304]{2,1,0:T(8,128)(2,1)}, u32[]{:S(2)}, u32[]{:S(2)}) async-start(bf16[16,128,2304]{2,1,0:T(8,128)(2,1)} %stack.2), calls=%async_computation.2 | async-start | bytes 18874368 | tf_op jit(solution)/shard_map/all_to_all | solution.py:41
  106.6 44.0 %all-gather.3.cloned.1.call-done = bf16[1024,2048]{0,1:T(8,128)(2,1)} async-done(((bf16[128,2048]{0,1:T(8,128)(2,1)}), bf16[1024,2048]{0,1:T(8,128)(2,1)}) %all-gather.3.cloned.1.call-update) | async-done | bytes 4194320 | tf_op jit(solution)/shard_map/all_gather | solution.py:142
  150.6 3.6 convolution_convert_fusion.1
  154.8 0.9 fusion.23
  155.7 34.9 %all-gather.5.cloned.1.call-done = bf16[768,2048]{1,0:T(8,128)(2,1)} async-done(((bf16[96,2048]{1,0:T(8,128)(2,1)}), bf16[768,2048]{1,0:T(8,128)(2,1)}) %all-gather.5.cloned.1.call-update) | async-done | bytes 3145744 | tf_op jit(solution)/shard_map/all_gather | solution.py:151
  190.6 321.3 %all-to-all-done.2 = bf16[16,128,2304]{2,1,0:T(8,128)(2,1)} async-done(((bf16[16,128,2304]{2,1,0:T(8,128)(2,1)}), bf16[16,128,2304]{2,1,0:T(8,128)(2,1)}, u32[]{:S(2)}, u32[]{:S(2)}) %all-to-all-start.2) | async-done | bytes 9437216 | tf_op jit(solution)/shard_map/all_to_all | solution.py:41
  511.9 7.0 %fusion.3 = f32[768,768]{1,0:T(8,128)} fusion(bf16[768,2048]{1,0:T(8,128)(2,1)} %all-gather.5.cloned.1.call-done, bf16[2048,2304]{1,0:T(8,128)(2,1)} %bitcast.19), kind=kOutput, calls=%fused_computation.4 | convolution fusion | flops 2415919104 | bytes 8650752 | tf_op jit(solution)/shard_map/dot_general | solution.py:152
  518.8 11.0 %convolution_convert_fusion = bf16[768,2048]{1,0:T(8,128)(2,1)} fusion(bf16[2048,2304]{1,0:T(8,128)(2,1)} %bitcast.19, f32[768,768]{1,0:T(8,128)} %fusion.3, bf16[768,2048]{1,0:T(8,128)(2,1)S(1)} %copy-done.11), kind=kOutput, calls=%fused_computation | convolution fusion | flops 4836950016 | bytes 14942208 | tf_op jit(solution)/shard_map/dot_general | solution.py:157
  529.8 42.4 %all_to_all.31 = bf16[8,96,2048]{2,1,0:T(8,128)(2,1)S(1)} all-to-all(bf16[8,96,2048]{2,1,0:T(8,128)(2,1)} %bitcast.85), channel_id=1, replica_groups=mesh['grp'=2,'sp'=16,'tp'=8] {'tp'}, dimensions={0} | all-to-all | bytes 6291456 | tf_op jit(solution)/shard_map/all_to_all | solution.py:61
  572.2 1.4 reduce_sum.54
  573.6 1.2 fusion.18
  574.8 2.0 fusion.24
  (62 shorter events, 10.4 us)
Async XLA Ops:
  6.5 23.8 %copy-start.10 = (f32[2]{0:T(128)S(1)}, f32[2]{0:T(128)}, u32[]{:S(2)}) copy-start(f32[2]{0:T(128)} %param.17) | copy-start | bytes 28
  7.3 21.7 %collective-permute-start.2 = (bf16[128,64]{0,1:T(8,128)(2,1)S(1)}, bf16[128,64]{0,1:T(8,128)(2,1)S(1)}, u32[]{:S(2)}, u32[]{:S(2)}) collective-permute-start(bf16[128,64]{0,1:T(8,128)(2,1)S(1)} %slice.52), channel_id=1, source_target_pairs={{0,8},{8,16},{16,24},{24,32},{32,40},{40,48},{48,56},{56,64},{64,7... | collective-permute-start | bytes 49160 | tf_op jit(solution)/shard_map/ppermute | solution.py:15
  13.2 12.6 %collective-permute-start.1 = (s32[128]{0:T(128)S(1)}, s32[128]{0:T(128)S(1)}, u32[]{:S(2)}, u32[]{:S(2)}) collective-permute-start(s32[128]{0:T(128)S(1)} %slice.49), channel_id=1, source_target_pairs={{0,8},{8,16},{16,24},{24,32},{32,40},{40,48},{48,56},{56,64},{64,7... | collective-permute-start | bytes 1544 | tf_op jit(solution)/shard_map/ppermute | solution.py:15
  18.4 12.4 %collective-permute-start = (bf16[128,64]{0,1:T(8,128)(2,1)S(1)}, bf16[128,64]{0,1:T(8,128)(2,1)S(1)}, u32[]{:S(2)}, u32[]{:S(2)}) collective-permute-start(bf16[128,64]{0,1:T(8,128)(2,1)S(1)} %slice.45), channel_id=1, source_target_pairs={{0,8},{8,16},{16,24},{24,32},{32,40},{40,48},{48,56},{56,64},{64,7... | collective-permute-start | bytes 49160 | tf_op jit(solution)/shard_map/ppermute | solution.py:15
  25.8 4.9 copy-start.1
  30.6 15.4 %copy-start.6 = (bf16[128,128]{1,0:T(8,128)(2,1)S(1)}, bf16[128,128]{1,0:T(8,128)(2,1)}, u32[]{:S(2)}) copy-start(bf16[128,128]{1,0:T(8,128)(2,1)} %param.18) | copy-start | bytes 98308
  30.8 35.1 %copy-start.4 = (bf16[128,768]{1,0:T(8,128)(2,1)S(1)}, bf16[128,768]{1,0:T(8,128)(2,1)}, u32[]{:S(2)}) copy-start(bf16[128,768]{1,0:T(8,128)(2,1)} %param.24) | copy-start | bytes 589828
  31.2 34.8 %copy-start.5 = (bf16[128,768]{1,0:T(8,128)(2,1)S(1)}, bf16[128,768]{1,0:T(8,128)(2,1)}, u32[]{:S(2)}) copy-start(bf16[128,768]{1,0:T(8,128)(2,1)} %param.23) | copy-start | bytes 589828
  31.2 35.0 %copy-start.3 = (bf16[768,128]{1,0:T(8,128)(2,1)S(1)}, bf16[768,128]{1,0:T(8,128)(2,1)}, u32[]{:S(2)}) copy-start(bf16[768,128]{1,0:T(8,128)(2,1)} %param.25) | copy-start | bytes 589828
  32.5 19.4 %all-to-all-start = ((bf16[8,96,128]{2,1,0:T(8,128)(2,1)}), bf16[8,96,128]{2,1,0:T(8,128)(2,1)S(1)}, u32[]{:S(2)}, u32[]{:S(2)}) async-start(bf16[8,96,128]{2,1,0:T(8,128)(2,1)} %reshape.177), calls=%async_computation | async-start | bytes 393216 | tf_op jit(solution)/shard_map/all_to_all | solution.py:139
  52.8 35.9 %all-to-all-start.1 = ((bf16[16,128,128]{1,2,0:T(8,128)(2,1)}), bf16[16,128,128]{1,2,0:T(8,128)(2,1)S(1)}, u32[]{:S(2)}, u32[]{:S(2)}) async-start(bf16[16,128,128]{1,2,0:T(8,128)(2,1)} %broadcast_in_dim.16), calls=%async_computation.1 | async-start | bytes 1048576 | tf_op jit(solution)/shard_map/all_to_all | solution.py:20
  88.7 4.6 copy-start
  93.3 418.6 %all-to-all-start.2 = ((bf16[16,128,2304]{2,1,0:T(8,128)(2,1)}), bf16[16,128,2304]{2,1,0:T(8,128)(2,1)}, u32[]{:S(2)}, u32[]{:S(2)}) async-start(bf16[16,128,2304]{2,1,0:T(8,128)(2,1)} %stack.2), calls=%async_computation.2 | async-start | bytes 18874368 | tf_op jit(solution)/shard_map/all_to_all | solution.py:41
  105.5 45.1 %all-gather.3.cloned.1.call-start = ((), (), s32[]{:S(2)}) async-start(), calls=%async_computation.4 | async-start | bytes 4718592 | tf_op jit(solution)/shard_map/all_gather | solution.py:142
  106.3 48.1 %copy-start.2 = (bf16[96,2048]{1,0:T(8,128)(2,1)S(1)}, bf16[96,2048]{1,0:T(8,128)(2,1)}, u32[]{:S(2)}) copy-start(bf16[96,2048]{1,0:T(8,128)(2,1)} %param.19) | copy-start | bytes 1179652
  106.3 48.1 %copy-start.7 = (f32[2048]{0:T(1024)S(1)}, f32[2048]{0:T(1024)}, u32[]{:S(2)}) copy-start(f32[2048]{0:T(1024)} %param.20) | copy-start | bytes 24580
  106.3 48.5 %copy-start.8 = (f32[2048]{0:T(1024)S(1)}, f32[2048]{0:T(1024)}, u32[]{:S(2)}) copy-start(f32[2048]{0:T(1024)} %param.21) | copy-start | bytes 24580
  106.3 84.3 %all-gather.5.cloned.1.call-start = ((), (), s32[]{:S(2)}) async-start(), calls=%async_computation.5 | async-start | bytes 3538944 | tf_op jit(solution)/shard_map/all_gather | solution.py:151
  511.9 7.0 %copy-start.11 = (bf16[768,2048]{1,0:T(8,128)(2,1)S(1)}, bf16[768,2048]{1,0:T(8,128)(2,1)}, u32[]{:S(2)}) copy-start(bf16[768,2048]{1,0:T(8,128)(2,1)} %all-gather.5.cloned.1.call-done) | copy-start | bytes 9437188
  572.2 2.6 copy-start.9
Sparse Core Ops, SparseCore 0:
  108.1 42.3 all-gather.2
  155.9 34.7 all-gather.4
